TPU v7x, 32 devices: a whole 2x2x4 slice. The times are simulated.
32 devices in a mesh: sp: 16 (over z, y, x), tp: 2 (over core).
Axes of the slice: x: 2, y: 2, z: 4, core: 2. Of those that a mesh axis runs over, the one named last changes fastest.
Arguments:
- tokens: bfloat16 [16384, 2048], P(('sp', 'tp')), may hold values from -6 to 6
- norm_gain: float32 [2048], replicated, may hold values from 0.1 to 1.9
- w_query: bfloat16 [2048, 1024], P('sp', 'tp'), may hold values from -0.125 to 0.125
- w_key: bfloat16 [2048, 1024], P('sp', 'tp'), may hold values from -0.125 to 0.125
- w_value: bfloat16 [2048, 1024], P('sp', 'tp'), may hold values from -0.125 to 0.125
- decay_rate: float32 [128, 8], P('sp', 'tp'), may hold values from 3.0517578e-06 to 0.1, as said below
- state_init: float32 [8, 128, 128], P('tp'), may hold values from -48 to 48
- out_gain: float32 [1024], P('tp'), may hold values from 0.1 to 1.9
- w_out: bfloat16 [1024, 2048], P('tp', 'sp'), may hold values from -0.1875 to 0.1875
Outputs:
- mixed: bfloat16 [16384, 2048], P(('sp', 'tp'))
Inputs may be any that keep to these rules, and one draw needn't show every extreme that they name: `decay_rate`: constant over each block of 128 positions.
All inputs are finite; a program needn't handle non-finite values.
Results may differ from a plain program's by a relative error of at most 0.025.
Values may be sent and summed in bfloat16 or wider, within the bound.
A program may use at most 64 MiB of HBM per device.

v0:
```python
import jax
import jax.numpy as jnp
from jax import lax
from jax.sharding import PartitionSpec as P

HEAD_DIM = 128
BLOCK = 128


EPS = 0.1
ROPE_BASE = 10000.0


def carried_in(shard, axis, combine, identity):
    count, index = (lax.axis_size(axis), lax.axis_index(axis))
    everything = jax.tree.map(
        lambda part, kind: lax.all_gather(part.astype(kind), axis),
        shard,
        (jnp.bfloat16, jnp.bfloat16),
    )
    start = jax.tree.map(
        lambda part, zero: jnp.broadcast_to(jnp.asarray(zero, part.dtype), part.shape),
        shard,
        identity,
    )

    def step(k, before):
        reached = k < index
        new = combine(
            before, jax.tree.map(lambda part, own: part[k].astype(own.dtype), everything, shard)
        )
        return jax.tree.map(lambda a, b: jnp.where(reached, a, b), new, before)

    return lax.fori_loop(0, count, step, start)


def rotate(values_in, positions):
    half_dim = values_in.shape[-1] // 2
    inv_freq = ROPE_BASE ** (-jnp.arange(half_dim, dtype=jnp.float32) / half_dim)
    angles = positions[:, None] * inv_freq[None, :]
    cosine = jnp.cos(angles)[:, None, :]
    sine_part = jnp.sin(angles)[:, None, :]
    first_half = values_in[..., :half_dim]
    second_half = values_in[..., half_dim:]
    return jnp.concatenate(
        [
            first_half * cosine - second_half * sine_part,
            second_half * cosine + first_half * sine_part,
        ],
        axis=-1,
    )


def block_terms(q_blocks, k_blocks, v_blocks, rate_blocks):
    high = lax.Precision.HIGHEST
    block_rows = q_blocks.shape[1]
    offsets = jnp.arange(block_rows, dtype=jnp.float32)
    step_gap = offsets[:, None] - offsets[None, :]
    inside = jnp.where(
        step_gap[None, None] >= 0.0,
        jnp.exp(-jnp.maximum(step_gap, 0.0)[None, None] * rate_blocks[:, :, None, None]),
        0.0,
    )
    scores = jnp.einsum("bihd,bjhd->bhij", q_blocks, k_blocks, precision=high) * inside
    inner_part = jnp.einsum("bhij,bjhe->bihe", scores, v_blocks, precision=high)
    tail_decay = jnp.exp(-(block_rows - 1.0 - offsets)[None, :, None] * rate_blocks[:, None, :])
    block_kv = jnp.einsum(
        "bjhd,bjhe->bhde", k_blocks * tail_decay[..., None], v_blocks, precision=high
    )
    block_decay = jnp.exp(-block_rows * rate_blocks)
    read_decay = jnp.exp(-(offsets + 1.0)[None, :, None] * rate_blocks[:, None, :])
    return (inner_part, block_kv, block_decay, read_decay)


def carry_states(block_kv, block_decay, start_state):

    def advance(state_now, block_item):
        return (block_item[1][:, None, None] * state_now + block_item[0], state_now)

    return lax.scan(advance, start_state, (block_kv, block_decay))


def read_out(q_blocks, prev_states, read_decay):
    return (
        jnp.einsum("bihd,bhde->bihe", q_blocks, prev_states, precision=lax.Precision.HIGHEST)
        * read_decay[..., None]
    )


def shards(tokens, norm_gain, w_query, w_key, w_value, decay_rate, state_init, out_gain, w_out):
    values_in = tokens.astype(jnp.float32)
    normed = (
        values_in
        * lax.rsqrt(jnp.mean(values_in * values_in, axis=-1, keepdims=True) + EPS)
        * norm_gain
    ).astype(jnp.bfloat16)
    head_cols = w_query.shape[1]
    heads_here = head_cols // HEAD_DIM
    query_all, key_all, value_all = (
        lax.all_gather(w_query, "sp", axis=0, tiled=True),
        lax.all_gather(w_key, "sp", axis=0, tiled=True),
        lax.all_gather(w_value, "sp", axis=0, tiled=True),
    )
    piece_rows = lax.all_gather(normed, "tp", axis=0, tiled=True)
    joined = jnp.concatenate(
        [
            jnp.dot(piece_rows, query_all, preferred_element_type=jnp.float32),
            jnp.dot(piece_rows, key_all, preferred_element_type=jnp.float32),
            jnp.dot(piece_rows, value_all, preferred_element_type=jnp.float32),
        ],
        axis=1,
    )
    query_raw = joined[:, :head_cols]
    key_raw = joined[:, head_cols : 2 * head_cols]
    value_raw = joined[:, 2 * head_cols :]
    span_rows = query_raw.shape[0]
    positions = (lax.axis_index("sp") * span_rows + jnp.arange(span_rows, dtype=jnp.int32)).astype(
        jnp.float32
    )
    query_rot = rotate(query_raw.reshape(span_rows, heads_here, HEAD_DIM), positions).astype(
        jnp.bfloat16
    )
    key_rot = rotate(key_raw.reshape(span_rows, heads_here, HEAD_DIM), positions).astype(
        jnp.bfloat16
    )
    value_rows = value_raw.astype(jnp.bfloat16)
    count_blocks = span_rows // BLOCK
    q_blocks = query_rot.astype(jnp.float32).reshape(count_blocks, BLOCK, heads_here, HEAD_DIM)
    k_blocks = key_rot.astype(jnp.float32).reshape(
        count_blocks, BLOCK, heads_here, HEAD_DIM
    ) * HEAD_DIM ** (-0.5)
    v_blocks = value_rows.astype(jnp.float32).reshape(count_blocks, BLOCK, heads_here, HEAD_DIM)
    inner_part, block_kv, block_decay, read_decay = block_terms(
        q_blocks, k_blocks, v_blocks, decay_rate
    )
    zero_state = jnp.zeros((heads_here, HEAD_DIM, HEAD_DIM), jnp.float32)
    total_decay = jnp.exp(-BLOCK * jnp.sum(decay_rate, axis=0))

    def combine(earlier, latter):
        return (earlier[0] * latter[0], latter[0][:, None, None] * earlier[1] + latter[1])

    identity = (jnp.ones((heads_here,), jnp.float32), zero_state)
    local_end = carry_states(block_kv, block_decay, zero_state)[0]
    before_decay, before_state = carried_in((total_decay, local_end), "sp", combine, identity)
    incoming = before_state + before_decay[:, None, None] * state_init
    prev_states = carry_states(block_kv, block_decay, incoming)[1]
    mixed_heads = inner_part + read_out(q_blocks, prev_states, read_decay)
    out_heads = mixed_heads.reshape(span_rows, heads_here, HEAD_DIM)
    out_heads = out_heads * lax.rsqrt(jnp.mean(out_heads * out_heads, axis=-1, keepdims=True) + EPS)
    out_heads = out_heads * out_gain.reshape(heads_here, HEAD_DIM)
    hidden = out_heads.reshape(span_rows, head_cols).astype(jnp.bfloat16)
    out_whole = lax.all_gather(w_out, "sp", axis=1, tiled=True)
    return lax.psum_scatter(
        jnp.dot(hidden, out_whole, preferred_element_type=jnp.float32).astype(jnp.bfloat16),
        "tp",
        scatter_dimension=0,
        tiled=True,
    )


def solution(mesh):
    in_specs = (
        P(("sp", "tp"), None),
        P(),
        P("sp", "tp"),
        P("sp", "tp"),
        P("sp", "tp"),
        P("sp", "tp"),
        P("tp", None, None),
        P("tp"),
        P("tp", "sp"),
    )
    out_specs = P(("sp", "tp"), None)
    return jax.shard_map(shards, mesh=mesh, in_specs=in_specs, out_specs=out_specs, check_vma=False)
```

profile of v0, /device:TPU:1, one launch (start us, length us, event | category | flops | bytes accessed | tf_op | source)
XLA Modules:
  0.0 372.6 jit_solution(2836490808201767689)
XLA Ops:
  7.3 2.1 fusion.2
  13.9 57.8 %all-gather.13.cloned.1.call-done = bf16[2048,512]{1,0:T(8,128)(2,1)} async-done(((bf16[128,512]{1,0:T(8,128)(2,1)}), bf16[2048,512]{1,0:T(8,128)(2,1)}) %all-gather.13.cloned.1.call-update) | async-done | bytes 2097168 | tf_op jit(solution)/shard_map/all_gather | solution.py:100
  71.6 15.4 %all-gather.9.cloned.1.call-done = bf16[1024,2048]{1,0:T(8,128)(2,1)} async-done(((bf16[512,2048]{1,0:T(8,128)(2,1)}), bf16[1024,2048]{1,0:T(8,128)(2,1)}) %all-gather.9.cloned.1.call-update) | async-done | bytes 4194320 | tf_op jit(solution)/shard_map/all_gather | solution.py:104
  87.0 5.2 %fusion.29 = f32[1024,512]{0,1:T(8,128)S(1)} fusion(bf16[1024,2048]{1,0:T(8,128)(2,1)} %all-gather.9.cloned.1.call-done, bf16[2048,512]{1,0:T(8,128)(2,1)} %all-gather.13.cloned.1.call-done), kind=kOutput, calls=%fused_computation.69 | convolution fusion | flops 2147483648 | bytes 8388608 | tf_op jit(solution)/shard_map/dot_general | solution.py:107
  92.2 57.8 %all-gather.15.cloned.1.call-done = bf16[2048,512]{1,0:T(8,128)(2,1)} async-done(((bf16[128,512]{1,0:T(8,128)(2,1)}), bf16[2048,512]{1,0:T(8,128)(2,1)}) %all-gather.15.cloned.1.call-update) | async-done | bytes 2097168 | tf_op jit(solution)/shard_map/all_gather | solution.py:101
  150.1 5.2 %fusion.30 = f32[1024,512]{0,1:T(8,128)S(1)} fusion(bf16[1024,2048]{1,0:T(8,128)(2,1)} %all-gather.9.cloned.1.call-done, bf16[2048,512]{1,0:T(8,128)(2,1)} %all-gather.15.cloned.1.call-done), kind=kOutput, calls=%fused_computation.70 | convolution fusion | flops 2147483648 | bytes 8388608 | tf_op jit(solution)/shard_map/dot_general | solution.py:108
  155.3 1.9 subtract_convert_fusion.1
  159.9 52.0 %all-gather.11.cloned.1.call-done = bf16[2048,512]{1,0:T(8,128)(2,1)} async-done(((bf16[128,512]{1,0:T(8,128)(2,1)}), bf16[2048,512]{1,0:T(8,128)(2,1)}) %all-gather.11.cloned.1.call-update) | async-done | bytes 2097168 | tf_op jit(solution)/shard_map/all_gather | solution.py:102
  211.9 5.2 %convolution_convert_fusion.1 = bf16[1024,512]{1,0:T(8,128)(2,1)S(1)} fusion(bf16[1024,2048]{1,0:T(8,128)(2,1)} %all-gather.9.cloned.1.call-done, bf16[2048,512]{1,0:T(8,128)(2,1)} %all-gather.11.cloned.1.call-done), kind=kOutput, calls=%fused_computation.33 | convolution fusion | flops 2148007936 | bytes 7340032 | tf_op jit(solution)/shard_map/dot_general | solution.py:109
  218.2 4.2 %fusion.6 = f32[8,4,128,128]{3,2,1,0:T(8,128)S(1)} fusion(f32[8,128,4]{1,2,0:T(4,128)S(1)} %get-tuple-element.245, bf16[8,128,4,128]{3,2,1,0:T(4,128)(2,1)} %reshape.189, bf16[8,128,4,64]{3,1,2,0:T(8,128)(2,1)} %copy.30, bf16[8,128,4,64]{3,1,2,0:T(8,128)(2,1)S(1)} %copy.29), kind=kOutput, calls=%fused_computation.21 | convolution fusion | flops 807927808 | bytes 4210688 | tf_op jit(solution)/shard_map/bjhd,bjhe->bhde/dot_general | solution.py:67
  226.7 32.7 %all-reduce = bf16[64]{0:T(256)(128)(2,1)S(1)} all-reduce(bf16[64]{0:T(256)(128)(2,1)S(1)} %dynamic-update-slice), channel_id=2, replica_groups=mesh['sp'=16,'tp'=2] {'sp'}, use_global_device_ids=true, to_apply=%add | all-reduce | flops 64 | bytes 256
  259.5 1.9 copy.41
  261.4 2.4 copy.27
  263.9 1.9 copy.42
  265.8 2.5 copy.28
  268.4 5.0 %fusion.5 = f32[8,4,128,128]{3,2,1,0:T(8,128)S(1)} fusion(bf16[8,128,4,64]{3,1,2,0:T(8,128)(2,1)} %copy.30, bf16[8,128,4,64]{3,1,2,0:T(8,128)(2,1)S(1)} %copy.29, bf16[8,128,4,64]{3,1,2,0:T(8,128)(2,1)} %copy.28, bf16[8,128,4,64]{3,1,2,0:T(8,128)(2,1)} %copy.27), kind=kOutput, calls=%fused_computation.20 | convolution fusion | flops 810024960 | bytes 4194304 | tf_op jit(solution)/shard_map/bihd,bjhd->bhij/dot_general | solution.py:64
  273.3 4.0 %fusion.10 = f32[8,4,128,128]{3,2,1,0:T(8,128)} fusion(f32[8,4,128,128]{3,2,1,0:T(8,128)S(1)} %fusion.5, f32[8,4]{1,0:T(8,128)S(1)} %copy.31, f32[128,128]{1,0:T(8,128)S(1)} %maximum_negate_fusion, pred[128,128]{1,0:T(8,128)(4,1)S(1)} %fusion.23, bf16[8,128,4,128]{3,2,1,0:T(4,128)(2,1)S(1)} %copy-done), kind=kOutput, calls=%fused_computation.28 | convolution fusion | flops 806879232 | bytes 5324928 | tf_op jit(solution)/shard_map/bhij,bjhe->bihe/dot_general | solution.py:65
  277.3 6.3 %all-gather.19.cloned.1.call-done = bf16[64,128,128]{2,1,0:T(8,128)(2,1)} async-done(((bf16[4,128,128]{2,1,0:T(8,128)(2,1)}), bf16[64,128,128]{2,1,0:T(8,128)(2,1)}) %all-gather.19.cloned.1.call-update) | async-done | bytes 2097168 | tf_op jit(solution)/shard_map/all_gather | solution.py:17
  283.6 16.9 %while.44 = (s32[]{:T(128)}, f32[4]{0:T(128)S(1)}, f32[4,128,128]{2,1,0:T(8,128)S(1)}, s32[]{:T(128)}, bf16[16,4]{1,0:T(8,128)(2,1)S(1)}, /*index=5*/bf16[16,4,128,128]{3,2,1,0:T(8,128)(2,1)}) while((s32[]{:T(128)}, f32[4]{0:T(128)S(1)}, f32[4,128,128]{2,1,0:T(8,128)S(1)}, s32[]{:T(128)}, bf16[16,4]{1,0:T(8,128)(2,1)S(1)}, ...), condition=%wide.region_5.6_spmd.clone.clone, body=%wide.region_4.5_spmd.clone.sunk.clone | while | flops 327700 | bytes 655531 | solution.py:34
  300.7 7.1 %while.42 = (s32[]{:T(128)}, f32[4,128,128]{2,1,0:T(8,128)S(1)}, f32[8,4,128,128]{3,2,1,0:T(8,128)}, f32[8,4]{1,0:T(8,128)S(1)}, f32[8,4,128,128]{3,2,1,0:T(8,128)S(1)}) while((s32[]{:T(128)}, f32[4,128,128]{2,1,0:T(8,128)S(1)}, f32[8,4,128,128]{3,2,1,0:T(8,128)}, f32[8,4]{1,0:T(8,128)S(1)}, ...), condition=%wide.region_7.8_spmd.clone, body=%wide.region_6.7_spmd.sunk.clone | while | flops 131074 | bytes 1311349 | solution.py:80
  307.9 4.8 %multiply_reduce_fusion = (f32[8,128,4]{1,2,0:T(4,128)S(1)}, f32[8,128,4,128]{1,3,2,0:T(8,128)S(1)}) fusion(f32[8,128,4]{1,2,0:T(4,128)S(1)} %get-tuple-element.244, f32[8,4,128,128]{3,2,1,0:T(8,128)} %get-tuple-element.167, bf16[8,128,4,64]{3,1,2,0:T(8,128)(2,1)} %copy.28, bf16[8,128,4,64]{3,1,2,0:T(8,128)(2,1)S(1)} %copy-done.1, ...), kind=kOutput, calls=%fused_computation.27 | convolution fusion | flops 809496576 | bytes 7372800 | tf_op jit(solution)/shard_map/bihd,bhde->bihe/dot_general | solution.py:85
  314.3 33.8 %all-gather.17.cloned.1.call-done = bf16[512,2048]{1,0:T(8,128)(2,1)} async-done(((bf16[512,128]{1,0:T(8,128)(2,1)}), bf16[512,2048]{1,0:T(8,128)(2,1)}) %all-gather.17.cloned.1.call-update) | async-done | bytes 2097168 | tf_op jit(solution)/shard_map/all_gather | solution.py:152
  348.1 5.9 %convolution_convert_fusion = bf16[1024,2048]{1,0:T(8,128)(2,1)} fusion(bf16[1024,512]{0,1:T(8,128)(2,1)S(1)} %fusion.8, bf16[512,2048]{1,0:T(8,128)(2,1)} %all-gather.17.cloned.1.call-done), kind=kOutput, calls=%fused_computation.17 | convolution fusion | flops 2149580800 | bytes 7340032 | tf_op jit(solution)/shard_map/dot_general | solution.py:154
  354.1 11.7 %reduce-scatter.2.cloned.1.call-done = bf16[512,2048]{1,0:T(8,128)(2,1)} async-done(((bf16[1024,2048]{1,0:T(8,128)(2,1)}), bf16[512,2048]{1,0:T(8,128)(2,1)}) %reduce-scatter.2.cloned.1.call-update) | async-done | bytes 2097168 | tf_op jit(solution)/shard_map/reduce_scatter | solution.py:153
  (136 shorter events, 38.3 us)
Async XLA Ops:
  6.5 2.9 copy-start.2
  6.5 2.9 copy-start.5
  6.5 65.1 %all-gather.13.cloned.1.call-start = ((), (), s32[]{:S(2)}) async-start(), calls=%async_computation.3 | async-start | bytes 2228224 | tf_op jit(solution)/shard_map/all_gather | solution.py:100
  7.3 79.7 %all-gather.9.cloned.1.call-start = ((), (), s32[]{:S(2)}) async-start(), calls=%async_computation.1 | async-start | bytes 6291456 | tf_op jit(solution)/shard_map/all_gather | solution.py:104
  11.3 1.4 copy-start.6
  11.3 138.8 %all-gather.15.cloned.1.call-start = ((), (), s32[]{:S(2)}) async-start(), calls=%async_computation.4 | async-start | bytes 2228224 | tf_op jit(solution)/shard_map/all_gather | solution.py:101
  12.0 199.8 %all-gather.11.cloned.1.call-start = ((), (), s32[]{:S(2)}) async-start(), calls=%async_computation.2 | async-start | bytes 2228224 | tf_op jit(solution)/shard_map/all_gather | solution.py:102
  12.6 271.0 %all-gather.19.cloned.1.call-start = ((), (), s32[]{:S(2)}) async-start(), calls=%async_computation.7 | async-start | bytes 2228224 | tf_op jit(solution)/shard_map/all_gather | solution.py:17
  157.2 1.0 copy-start.3
  222.4 2.7 copy-start.8
  224.2 123.9 %all-gather.17.cloned.1.call-start = ((), (), s32[]{:S(2)}) async-start(), calls=%async_computation.5 | async-start | bytes 2228224 | tf_op jit(solution)/shard_map/all_gather | solution.py:152
  224.8 140.9 %reduce-scatter.2.cloned.1.call-start = ((), (), s32[]{:S(2)}) async-start(), calls=%async_computation.6 | async-start | bytes 6291456 | tf_op jit(solution)/shard_map/reduce_scatter | solution.py:153
  268.3 5.0 %copy-start = (bf16[8,128,4,128]{3,2,1,0:T(4,128)(2,1)S(1)}, bf16[8,128,4,128]{3,2,1,0:T(4,128)(2,1)}, u32[]{:S(2)}) copy-start(bf16[8,128,4,128]{3,2,1,0:T(4,128)(2,1)} %reshape.189) | copy-start | bytes 3145732
  277.3 23.3 %copy-start.4 = (f32[4,128,128]{2,1,0:T(8,128)S(1)}, f32[4,128,128]{2,1,0:T(8,128)}, u32[]{:S(2)}) copy-start(f32[4,128,128]{2,1,0:T(8,128)} %param.21) | copy-start | bytes 786436
  300.7 7.1 %copy-start.1 = (bf16[8,128,4,64]{3,1,2,0:T(8,128)(2,1)S(1)}, bf16[8,128,4,64]{3,1,2,0:T(8,128)(2,1)}, u32[]{:S(2)}) copy-start(bf16[8,128,4,64]{3,1,2,0:T(8,128)(2,1)} %copy.27) | copy-start | bytes 1572868
  312.7 1.3 copy-start.7
Sparse Core Ops, SparseCore 0:
  10.1 61.4 all-gather.12
  73.2 13.7 all-gather.8
  89.8 60.2 all-gather.14
  152.7 59.1 all-gather.10
  224.3 59.2 all-gather.18
  286.2 61.8 all-gather.16
  354.2 11.5 reduce-scatter.1
where the time goes:
time: 373 us
  waiting for transfers between devices  237 us (64%)
  matrix products  39.5 us (11%)
  blocking collectives  32.7 us (9%)
  other arithmetic  26.5 us (7%)
  local copies, waits for them, and re-layouts  20.9 us (6%)
  between operations  14.5 us (4%)
    all_gather x1, waiting for transfers between devices, shards(): lax.all_gather(w_key, 'sp', axis=0, tiled=True)  57.8 us
    all_gather x1, waiting for transfers between devices, shards(): lax.all_gather(w_query, 'sp', axis=0, tiled=True)  57.8 us
    all_gather x1, waiting for transfers between devices, shards(): lax.all_gather(w_value, 'sp', axis=0, tiled=True)  52 us
    all_gather x1, waiting for transfers between devices, shards(): out_whole = lax.all_gather(w_out, 'sp', axis=1, tiled=True)  33.8 us
    unnamed x1, blocking collectives  32.7 us
    select_n x32, other arithmetic, step(): return jax.tree.map(lambda a, b: jnp.where(reached, a, b), new, before)  16.5 us
    all_gather x1, waiting for transfers between devices, shards(): piece_rows = lax.all_gather(normed, 'tp', axis=0, tiled=True)  15.4 us
    reduce_scatter x1, waiting for transfers between devices, shards(): lax.psum_scatter(jnp.dot(hidden, out_whole, preferred_element_type=jnp.fl...  11.7 us
  transfers between devices with their start and end apart: 7, of which 7 were waited for; matrix products, arithmetic and copies ran while one was open for 18% of the time, Pallas kernels for 0%

commit v1 on v0

v1 whole, which is shorter than its diff:
```python
import functools

import jax
import jax.numpy as jnp
from jax import lax
from jax.experimental import pallas as pl
from jax.experimental.pallas import tpu as pltpu
from jax.sharding import PartitionSpec as P

HEAD_DIM = 128
BLOCK = 128
EPS = 0.1
ROPE_BASE = 10000.0
MESH = pl.DeviceIdType.MESH
F32 = jnp.float32
BF16 = jnp.bfloat16


def remote(src, dst, send, recv, device):
    return pltpu.make_async_remote_copy(
        src_ref=src, dst_ref=dst, send_sem=send, recv_sem=recv, device_id=device, device_id_type=MESH
    )


class Gather:
    def __init__(self, buf, layers, place, sems):
        self.buf, self.layers, self.place = buf, layers, place
        self.z, self.y, self.x, self.tp = place
        self.rows = buf.shape[0] // (4 * layers)
        self.s_x, self.r_x, self.s_y, self.r_y, self.s_up, self.s_dn, self.r_z = sems

    def at(self, zi, yi, xi, piece=None):
        start = ((zi * 2 + yi) * 2 + xi) * self.rows
        if piece is None:
            return self.buf.at[pl.ds(pl.multiple_of(start, self.rows), self.rows)]
        half = self.rows // 2
        return self.buf.at[pl.ds(pl.multiple_of(start + piece * half, half), half)]

    def device(self, zi, yi, xi):
        return ((zi * 2 + yi) * 2 + xi, self.tp)

    def copy_x(self, zi, j):
        ref = self.at(zi, self.y if j < 2 else 1 - self.y, self.x, (0, 1, 0)[j])
        return remote(ref, ref, self.s_x.at[zi, j], self.r_x.at[zi, j],
                      self.device(self.z, self.y, 1 - self.x))

    def copy_y(self, zi, j):
        ref = self.at(zi, self.y, self.x if j < 2 else 1 - self.x, (1, 0, 1)[j])
        return remote(ref, ref, self.s_y.at[zi, j], self.r_y.at[zi, j],
                      self.device(self.z, 1 - self.y, self.x))

    def copy_z(self, zi, step):
        ref = self.at(zi, self.y, self.x)
        sem = self.s_up if step > 0 else self.s_dn
        return remote(ref, ref, sem.at[zi], self.r_z.at[zi],
                      self.device(self.z + step, self.y, self.x))

    def order(self, t):
        z, last = self.z, self.layers - 1
        near = z - (t + 1) // 2 if t % 2 else z + t // 2
        m = jnp.minimum(z, last - z)
        far = jnp.where(z < last - z, t, last - t)
        return jnp.where(t <= 2 * m, near, far)

    def column(self, t):
        zi = self.order(t)
        if t > 0:
            self.copy_z(zi, 1).wait_recv()
        self.copy_y(zi, 1).start()
        self.copy_x(zi, 1).start()

        @pl.when((zi <= self.z) & (self.z < self.layers - 1))
        def _():
            self.copy_z(zi, 1).start()

        @pl.when((zi >= self.z) & (self.z > 0))
        def _():
            self.copy_z(zi, -1).start()

        self.copy_x(zi, 0).start()
        self.copy_y(zi, 0).start()

    def cross(self, t):
        zi = self.order(t)
        self.copy_y(zi, 1).wait_recv()
        self.copy_x(zi, 2).start()
        self.copy_x(zi, 1).wait_recv()
        self.copy_y(zi, 2).start()

    def arrive(self, t):
        zi = self.order(t)
        for j in (0, 2):
            self.copy_x(zi, j).wait_recv()
            self.copy_y(zi, j).wait_recv()
        return zi

    def drain(self):
        for t in range(self.layers):
            zi = self.order(t)
            for j in range(3):
                self.copy_x(zi, j).wait_send()
                self.copy_y(zi, j).wait_send()

            @pl.when((zi <= self.z) & (self.z < self.layers - 1))
            def _():
                self.copy_z(zi, 1).wait_send()

            @pl.when((zi >= self.z) & (self.z > 0))
            def _():
                self.copy_z(zi, -1).wait_send()


def nt_dot(a, b):
    return lax.dot_general(a, b, (((1,), (1,)), ((), ())), preferred_element_type=F32)


def tn_dot(a, b):
    return lax.dot_general(a, b, (((0,), (0,)), ((), ())), preferred_element_type=F32)


def kernel(layers, peers, tokens, gain, wq, wk, wv, wo, rates, state_init, out_gain, freq, out,
           w_all, wo_all, normed, acc, cosine, sine, q_rot, k_rot, v_row, inner, prev, state,
           hidden, part, landed, own, tot_send, tot_recv, excl, excl_d, z_send, z_recv, incoming,
           local_sem, nrm_s, nrm_r, part_s, part_r, st_s, st_r, zs_s, zs_r, *gather_sems):
    me, tp = lax.axis_index("sp"), lax.axis_index("tp")
    z, y, x = me // 4, (me // 2) % 2, me % 2
    rows_here, width = tokens.shape
    span = rows_here * peers
    cols = wq.shape[1]
    heads = cols // HEAD_DIM
    blocks = span // BLOCK
    shard = wq.shape[0]
    gq = Gather(w_all, layers, (z, y, x, tp), gather_sems[:7])
    go = Gather(wo_all, layers, (z, y, x, tp), gather_sems[7:])

    mine = pl.ds(pl.multiple_of(me * shard, shard), shard)
    fills = [
        pltpu.make_async_copy(src, dst, local_sem.at[i])
        for i, (src, dst) in enumerate((
            (wq, w_all.at[mine, pl.ds(0, cols)]),
            (wk, w_all.at[mine, pl.ds(cols, cols)]),
            (wv, w_all.at[mine, pl.ds(2 * cols, cols)]),
            (wo, wo_all.at[mine]),
        ))
    ]
    for fill in fills:
        fill.start()

    barrier = pltpu.get_barrier_semaphore()

    def greet(device):
        pl.semaphore_signal(barrier, inc=1, device_id=device, device_id_type=MESH)

    greet(gq.device(z, y, 1 - x))
    greet(gq.device(z, 1 - y, x))
    for d in range(1, peers):
        greet((me, (tp + d) % peers))

    @pl.when(z > 0)
    def _():
        greet(gq.device(z - 1, y, x))

    @pl.when(z < layers - 1)
    def _():
        greet(gq.device(z + 1, y, x))

    pl.semaphore_wait(
        barrier, 1 + peers + jnp.minimum(z, 1) + jnp.minimum(layers - 1 - z, 1))

    for fill in fills:
        fill.wait()
    gq.column(0)

    base = pl.multiple_of(tp * rows_here, rows_here)
    tile = 64

    @pl.loop(0, rows_here // tile)
    def _(i):
        at = pl.ds(pl.multiple_of(i * tile, tile), tile)
        u = tokens[at, :].astype(F32)
        scale = lax.rsqrt(jnp.mean(u * u, axis=-1, keepdims=True) + EPS)
        normed[pl.ds(pl.multiple_of(base + i * tile, tile), tile), :] = (
            u * scale * gain[...]
        ).astype(BF16)

    def send_normed(d):
        ref = normed.at[pl.ds(base, rows_here)]
        return remote(ref, ref, nrm_s.at[d - 1], nrm_r.at[d - 1], (me, (tp + d) % peers))

    @pl.loop(0, span // BLOCK)
    def _(i):
        at = pl.ds(pl.multiple_of(i * BLOCK, BLOCK), BLOCK)
        pos = lax.broadcasted_iota(jnp.int32, (BLOCK, HEAD_DIM), 0) + (me * span + i * BLOCK)
        angle = pos.astype(F32) * freq[...]
        lane = lax.broadcasted_iota(jnp.int32, (BLOCK, HEAD_DIM), 1)
        sin = jnp.sin(angle)
        cosine[at, :] = jnp.cos(angle)
        sine[at, :] = jnp.where(lane < HEAD_DIM // 2, -sin, sin)

    for d in range(1, peers):
        send_normed(d).start()
    if layers > 1:
        gq.column(1)
    gq.cross(0)
    for d in range(1, peers):
        send_normed(d).wait_recv()

    deep = 4 * shard
    m_tile = 256

    def product(t):
        zi = gq.arrive(t)
        at_k = pl.ds(pl.multiple_of(zi * deep, deep), deep)

        @pl.loop(0, span // m_tile)
        def _(i):
            at = pl.ds(pl.multiple_of(i * m_tile, m_tile), m_tile)
            for c in range(3):
                at_c = pl.ds(c * cols, cols)
                term = jnp.dot(normed[at, at_k], w_all[at_k, at_c], preferred_element_type=F32)
                acc[at, at_c] = term if t == 0 else acc[at, at_c] + term

    for t in range(layers):
        if t + 2 < layers:
            gq.column(t + 2)
        else:
            go.column(t + 2 - layers)
        if t + 1 < layers:
            gq.cross(t + 1)
        product(t)

    gap = (lax.broadcasted_iota(jnp.int32, (BLOCK, BLOCK), 0)
           - lax.broadcasted_iota(jnp.int32, (BLOCK, BLOCK), 1)).astype(F32)
    row = lax.broadcasted_iota(jnp.int32, (BLOCK, HEAD_DIM), 0).astype(F32)

    for h in range(heads):
        state[h] = jnp.zeros((HEAD_DIM, HEAD_DIM), F32)

    def states(b, sums):
        at = pl.ds(pl.multiple_of(b * BLOCK, BLOCK), BLOCK)
        cos, sin = cosine[at, :], sine[at, :]
        new = []
        for h in range(heads):
            rate = rates[b, h]
            head = pl.ds(h * HEAD_DIM, HEAD_DIM)
            u = acc[at, pl.ds(h * HEAD_DIM, HEAD_DIM)]
            q = (u * cos + pltpu.roll(u, HEAD_DIM // 2, 1) * sin).astype(BF16)
            u = acc[at, pl.ds(cols + h * HEAD_DIM, HEAD_DIM)]
            k = (u * cos + pltpu.roll(u, HEAD_DIM // 2, 1) * sin).astype(BF16)
            v = acc[at, pl.ds(2 * cols + h * HEAD_DIM, HEAD_DIM)].astype(BF16)
            q_rot[at, head] = q
            k_rot[at, head] = k
            v_row[at, head] = v
            tail = jnp.exp(-(BLOCK - 1.0 - row) * rate) * HEAD_DIM ** (-0.5)
            kv = tn_dot((k.astype(F32) * tail).astype(BF16), v)
            now = state[h]
            prev[b, h] = now
            state[h] = jnp.exp(jnp.full((1, HEAD_DIM), -float(BLOCK), F32) * rate) * now + kv
            new.append(sums[h] + rate)
        return tuple(new)

    sums = lax.fori_loop(0, blocks, states, (jnp.float32(0.0),) * heads)

    def decay_of(total):
        return jnp.exp(jnp.full((1, HEAD_DIM), -float(BLOCK), F32) * total)

    def pair(step, h, device):
        return remote(tot_send.at[step, h], tot_recv.at[step, h], st_s.at[step, h],
                      st_r.at[step, h], device)

    x_dev, y_dev = gq.device(z, y, 1 - x), gq.device(z, 1 - y, x)
    up_dev = gq.device(z + 1, y, x)

    def put(step, h, decay, value):
        tot_send[step, h, :HEAD_DIM] = value.astype(BF16)
        tot_send[step, h, HEAD_DIM:] = jnp.broadcast_to(decay, (16, HEAD_DIM)).astype(BF16)

    def take(step, h):
        return (tot_recv[step, h, HEAD_DIM:].astype(F32)[:1], tot_recv[step, h, :HEAD_DIM].astype(F32))

    def both(high, decay, value, other):
        d_in, s_in = other
        late = jnp.where(high, decay, d_in)
        total = late * jnp.where(high, s_in, value) + jnp.where(high, value, s_in)
        return decay * d_in, total

    for h in range(heads):
        put(0, h, decay_of(sums[h]), state[h])
        pair(0, h, x_dev).start()

    def inside(b, carry):
        at = pl.ds(pl.multiple_of(b * BLOCK, BLOCK), BLOCK)
        for h in range(heads):
            rate = rates[b, h]
            head = pl.ds(h * HEAD_DIM, HEAD_DIM)
            fall = jnp.where(gap >= 0.0, jnp.exp(-jnp.maximum(gap, 0.0) * rate), 0.0)
            score = nt_dot(q_rot[at, head], k_rot[at, head]) * (fall * HEAD_DIM ** (-0.5))
            inner[at, head] = jnp.dot(score.astype(BF16), v_row[at, head], preferred_element_type=F32)
        return carry

    third = -(-blocks // 3)
    lax.fori_loop(0, third, inside, 0)
    for h in range(heads):
        pair(0, h, x_dev).wait_recv()
        got = take(0, h)
        excl[h] = jnp.where(x == 1, got[1], 0.0)
        excl_d[h] = jnp.broadcast_to(jnp.where(x == 1, got[0], 1.0), (8, HEAD_DIM))
        decay, value = both(x == 1, decay_of(sums[h]), state[h], got)
        put(1, h, decay, value)
        state[h] = value
        own_decay = jnp.broadcast_to(decay, (8, HEAD_DIM))
        incoming[h, :8] = own_decay
        pair(1, h, y_dev).start()
    lax.fori_loop(third, 2 * third, inside, 0)
    for h in range(heads):
        pair(1, h, y_dev).wait_recv()
        got = take(1, h)
        own_d, own_s = excl_d[h][:1], excl[h]
        excl[h] = jnp.where(y == 1, own_d * got[1] + own_s, own_s)
        excl_d[h] = jnp.broadcast_to(jnp.where(y == 1, own_d * got[0], own_d), (8, HEAD_DIM))
        decay, value = both(y == 1, incoming[h, :8][:1], state[h], got)
        state[h] = value

        def lift(h):
            return remote(z_send.at[h], z_recv.at[h], zs_s.at[h], zs_r.at[h], up_dev)

        @pl.when(z == 0)
        def _():
            incoming[h] = state_init[h]

        @pl.when(z > 0)
        def _():
            lift(h).wait_recv()
            incoming[h] = z_recv[h].astype(F32)

        @pl.when(z < layers - 1)
        def _():
            z_send[h] = (decay * incoming[h] + value).astype(BF16)
            lift(h).start()

        incoming[h] = excl_d[h][:1] * incoming[h] + excl[h]

    lax.fori_loop(2 * third, blocks, inside, 0)

    for t in range(layers):
        if t + 2 < layers:
            go.column(t + 2)
        go.cross(t)

    def finish(b, sums):
        at = pl.ds(pl.multiple_of(b * BLOCK, BLOCK), BLOCK)
        new = []
        for h in range(heads):
            rate = rates[b, h]
            head = pl.ds(h * HEAD_DIM, HEAD_DIM)
            before = prev[b, h] + decay_of(sums[h]) * incoming[h]
            read = jnp.exp(-(row + 1.0) * rate)
            kept = inner[at, head] + read * jnp.dot(
                q_rot[at, head], before.astype(BF16), preferred_element_type=F32)
            kept = kept * lax.rsqrt(jnp.mean(kept * kept, axis=-1, keepdims=True) + EPS)
            hidden[at, head] = (kept * out_gain[:, head]).astype(BF16)
            new.append(sums[h] + rate)
        return tuple(new)

    lax.fori_loop(0, blocks, finish, (jnp.float32(0.0),) * heads)
    for t in range(layers):
        go.arrive(t)

    o_tile = min(128, rows_here)

    def project(start, store):
        @pl.loop(0, rows_here // o_tile)
        def _(i):
            rows = pl.ds(pl.multiple_of(start + i * o_tile, o_tile), o_tile)
            store(pl.ds(pl.multiple_of(i * o_tile, o_tile), o_tile),
                  nt_dot(hidden[rows, :], wo_all[...]).astype(BF16))

    def hand(d):
        return remote(part.at[d - 1], landed.at[d - 1], part_s.at[d - 1], part_r.at[d - 1],
                      (me, (tp + d) % peers))

    for d in range(1, peers):
        def keep(at, value):
            part[d - 1, at, :] = value

        project(((tp + d) % peers) * rows_here, keep)
        hand(d).start()

    def keep_own(at, value):
        own[at, :] = value

    project(base, keep_own)
    for d in range(1, peers):
        hand(d).wait_recv()

    @pl.loop(0, rows_here // tile)
    def _(i):
        at = pl.ds(pl.multiple_of(i * tile, tile), tile)
        total = own[at, :].astype(F32)
        for d in range(1, peers):
            total = total + landed[d - 1, at, :].astype(F32)
        out[at, :] = total.astype(BF16)

    gq.drain()
    go.drain()
    for d in range(1, peers):
        send_normed(d).wait_send()
        hand(d).wait_send()
    for h in range(heads):
        pair(0, h, x_dev).wait_send()
        pair(1, h, y_dev).wait_send()

    @pl.when(z < layers - 1)
    def _():
        for h in range(heads):
            remote(z_send.at[h], z_recv.at[h], zs_s.at[h], zs_r.at[h], up_dev).wait_send()


def shards(tokens, norm_gain, w_query, w_key, w_value, decay_rate, state_init, out_gain, w_out):
    n_sp, peers = lax.axis_size("sp"), lax.axis_size("tp")
    layers = n_sp // 4
    rows_here, width = tokens.shape
    span = rows_here * peers
    cols = w_query.shape[1]
    heads = cols // HEAD_DIM
    blocks = span // BLOCK
    half = HEAD_DIM // 2
    freq = ROPE_BASE ** (-jnp.arange(half, dtype=F32) / half)
    freq = jnp.concatenate([freq, freq])[None]
    vmem = pl.BlockSpec(memory_space=pltpu.VMEM)
    hbm = pl.BlockSpec(memory_space=pl.ANY)
    smem = pl.BlockSpec(memory_space=pltpu.SMEM)
    dma = pltpu.SemaphoreType.DMA
    others = max(peers - 1, 1)
    gather_sems = [dma((layers, 3))] * 4 + [dma((layers,))] * 3
    v = pltpu.VMEM
    return pl.pallas_call(
        functools.partial(kernel, layers, peers),
        out_shape=jax.ShapeDtypeStruct((rows_here, width), BF16),
        in_specs=[vmem, vmem, hbm, hbm, hbm, hbm, smem, vmem, vmem, vmem],
        out_specs=vmem,
        scratch_shapes=[
            v((width, 3 * cols), BF16), v((width, cols), BF16), v((span, width), BF16),
            v((span, 3 * cols), F32), v((span, HEAD_DIM), F32), v((span, HEAD_DIM), F32),
            v((span, cols), BF16), v((span, cols), BF16), v((span, cols), BF16),
            v((span, cols), F32), v((blocks, heads, HEAD_DIM, HEAD_DIM), F32),
            v((heads, HEAD_DIM, HEAD_DIM), F32), v((span, cols), BF16),
            v((others, rows_here, width), BF16), v((others, rows_here, width), BF16),
            v((rows_here, width), BF16),
            v((2, heads, HEAD_DIM + 16, HEAD_DIM), BF16), v((2, heads, HEAD_DIM + 16, HEAD_DIM), BF16),
            v((heads, HEAD_DIM, HEAD_DIM), F32), v((heads, 8, HEAD_DIM), F32),
            v((heads, HEAD_DIM, HEAD_DIM), BF16), v((heads, HEAD_DIM, HEAD_DIM), BF16),
            v((heads, HEAD_DIM, HEAD_DIM), F32),
            dma((4,)), dma((others,)), dma((others,)), dma((others,)), dma((others,)),
            dma((2, heads)), dma((2, heads)), dma((heads,)), dma((heads,)),
        ] + gather_sems * 2,
        compiler_params=pltpu.CompilerParams(
            collective_id=0, has_side_effects=True, vmem_limit_bytes=62 * 1024 * 1024),
    )(tokens, norm_gain[None], w_query, w_key, w_value, w_out.T, decay_rate, state_init,
      out_gain[None], freq)


def solution(mesh):
    in_specs = (
        P(("sp", "tp"), None),
        P(),
        P("sp", "tp"),
        P("sp", "tp"),
        P("sp", "tp"),
        P("sp", "tp"),
        P("tp", None, None),
        P("tp"),
        P("tp", "sp"),
    )
    out_specs = P(("sp", "tp"), None)
    return jax.shard_map(shards, mesh=mesh, in_specs=in_specs, out_specs=out_specs, check_vma=False)
```

time: 373 us -> 115 us (0.31)
  waiting for transfers between devices: 237 us -> 0 us
  Pallas kernels: 0 us -> 108 us
  matrix products: 39.5 us -> 0 us
  blocking collectives: 32.7 us -> 0 us
  other arithmetic: 26.5 us -> 0.63 us
  local copies, waits for them, and re-layouts: 20.9 us -> 6.17 us
  between operations: 14.5 us -> 0.01 us
    all_gather x6 -> x0, waiting for transfers between devices: 223 us -> none  [the longest x1 57.8 us: shards(): lax.all_gather(w_key, 'sp', axis=0, tiled=True)]
    pallas_call x0 -> x1, Pallas kernels: none -> 108 us  [shards(): pl.pallas_call(functools.partial(kernel, layers, peers), out_shape=jax.Sh...]
    dot_general x8 -> x0, matrix products: 39.5 us -> none  [the longest x1 5.92 us: shards(): jnp.dot(hidden, out_whole, preferred_element_type=jnp.float32)]
    unnamed x1 -> x0, blocking collectives: 32.7 us -> none
    select_n x32 -> x0, other arithmetic: 16.5 us -> none  [step(): return jax.tree.map(lambda a, b: jnp.where(reached, a, b), new, before)]
    reduce_scatter x1 -> x0, waiting for transfers between devices: 11.7 us -> none  [shards(): lax.psum_scatter(jnp.dot(hidden, out_whole, preferred_element_type=jnp.fl...]
    concatenate x4 -> x0, local copies, waits for them, and re-layouts: 7.06 us -> none  [rotate(): jnp.concatenate([first_half * cosine - second_half * sine_part, second_ha...]
    dynamic_update_slice x8 -> x0, local copies, waits for them, and re-layouts: 5.83 us -> none  [carry_states(): return lax.scan(advance, start_state, (block_kv, block_decay))]
  transfers between devices with their start and end apart: 7 -> 0, of which waited for: 7 -> 0; matrix products, arithmetic and copies ran while one was open for 18% -> 0% of each run, Pallas kernels for 0% -> 0%
where the time goes in v1:
time: 115 us
  Pallas kernels  108 us (94%)
  local copies, waits for them, and re-layouts  6.17 us (5%)
    pallas_call x1, Pallas kernels, shards(): pl.pallas_call(functools.partial(kernel, layers, peers), out_shape=jax.Sh...  108 us
    unnamed x3, local copies, waits for them, and re-layouts  6.17 us

profile of v1, /device:TPU:1, one launch (start us, length us, event | category | flops | bytes accessed | tf_op | source)
XLA Modules:
  0.0 114.7 jit_solution(12055008419069077001)
XLA Ops:
  0.0 0.6 maximum_bitcast_fusion.freq
  0.6 1.3 %copy.11.rates = f32[8,4]{1,0:T(8,128)} copy(f32[8,4]{0,1:T(4,128)} %param.14) | data formatting | bytes 256 | tf_op args[5]
  2.0 1.7 %copy.10 = bf16[512,128]{0,1:T(8,128)(2,1)} copy(bf16[512,128]{1,0:T(8,128)(2,1)} %param.17) | data formatting | bytes 262144 | tf_op args[8]
  3.6 107.8 %shard_map.91 = bf16[512,2048]{1,0:T(8,128)(2,1)} custom-call(bf16[512,2048]{1,0:T(8,128)(2,1)} %tokens.1, f32[1,2048]{1,0:T(1,128)} %bitcast.6, bf16[128,512]{1,0:T(8,128)(2,1)} %wq.1, bf16[128,512]{1,0:T(8,128)(2,1)} %wk.1, bf16[128,512]{1,0:T(8,128)(2,1)} %wv.1, bf16[128,512]{1,0:T(8,128)(2,1)} %bitcast.5, f32[8,4]{1,0:T(8,128)} %copy.11.rates, ...), custom_call_target="tpu_custom_call" | custom-call | tf_op jit(solution)/shard_map/pallas_call | solution.py:437
  111.5 3.2 %copy.13 = bf16[512,2048]{1,0:T(8,128)(2,1)} copy(bf16[512,2048]{1,0:T(8,128)(2,1)} %shard_map.91) | data formatting | bytes 4194304
  (1 shorter events, 0.0 us)

commit v2 on v1

--- a/solution.py
+++ b/solution.py
@@ -119,8 +119,8 @@
 
 
 def kernel(layers, peers, tokens, gain, wq, wk, wv, wo, rates, state_init, out_gain, freq, out,
-           w_all, wo_all, normed, acc, cosine, sine, q_rot, k_rot, v_row, inner, prev, state,
-           hidden, part, landed, own, tot_send, tot_recv, excl, excl_d, z_send, z_recv, incoming,
+           wkv_all, wq_all, wo_all, normed, acc, cosine, sine, q_rot, k_rot, v_row, inner, prev, state,
+           hidden, part, landed, own, tot_send, tot_recv, excl, excl_d, plane_d, z_send, z_recv, incoming,
            local_sem, nrm_s, nrm_r, part_s, part_r, st_s, st_r, zs_s, zs_r, *gather_sems):
     me, tp = lax.axis_index("sp"), lax.axis_index("tp")
     z, y, x = me // 4, (me // 2) % 2, me % 2
@@ -130,16 +130,17 @@
     heads = cols // HEAD_DIM
     blocks = span // BLOCK
     shard = wq.shape[0]
-    gq = Gather(w_all, layers, (z, y, x, tp), gather_sems[:7])
-    go = Gather(wo_all, layers, (z, y, x, tp), gather_sems[7:])
+    gk = Gather(wkv_all, layers, (z, y, x, tp), gather_sems[:7])
+    gq = Gather(wq_all, layers, (z, y, x, tp), gather_sems[7:14])
+    go = Gather(wo_all, layers, (z, y, x, tp), gather_sems[14:])
 
     mine = pl.ds(pl.multiple_of(me * shard, shard), shard)
     fills = [
         pltpu.make_async_copy(src, dst, local_sem.at[i])
         for i, (src, dst) in enumerate((
-            (wq, w_all.at[mine, pl.ds(0, cols)]),
-            (wk, w_all.at[mine, pl.ds(cols, cols)]),
-            (wv, w_all.at[mine, pl.ds(2 * cols, cols)]),
+            (wq, wq_all.at[mine]),
+            (wk, wkv_all.at[mine, pl.ds(0, cols)]),
+            (wv, wkv_all.at[mine, pl.ds(cols, cols)]),
             (wo, wo_all.at[mine]),
         ))
     ]
@@ -169,7 +170,7 @@
 
     for fill in fills:
         fill.wait()
-    gq.column(0)
+    gk.column(0)
 
     base = pl.multiple_of(tp * rows_here, rows_here)
     tile = 64
@@ -187,8 +188,7 @@
         ref = normed.at[pl.ds(base, rows_here)]
         return remote(ref, ref, nrm_s.at[d - 1], nrm_r.at[d - 1], (me, (tp + d) % peers))
 
-    @pl.loop(0, span // BLOCK)
-    def _(i):
+    def trig(i, carry):
         at = pl.ds(pl.multiple_of(i * BLOCK, BLOCK), BLOCK)
         pos = lax.broadcasted_iota(jnp.int32, (BLOCK, HEAD_DIM), 0) + (me * span + i * BLOCK)
         angle = pos.astype(F32) * freq[...]
@@ -196,38 +196,48 @@
         sin = jnp.sin(angle)
         cosine[at, :] = jnp.cos(angle)
         sine[at, :] = jnp.where(lane < HEAD_DIM // 2, -sin, sin)
+        return carry
 
     for d in range(1, peers):
         send_normed(d).start()
-    if layers > 1:
-        gq.column(1)
-    gq.cross(0)
+    gk.column(1)
+    gk.cross(0)
+    if layers > 2:
+        gk.column(2)
     for d in range(1, peers):
         send_normed(d).wait_recv()
 
     deep = 4 * shard
     m_tile = 256
 
-    def product(t):
-        zi = gq.arrive(t)
+    def product(gather, t, first, count):
+        zi = gather.arrive(t)
         at_k = pl.ds(pl.multiple_of(zi * deep, deep), deep)
 
         @pl.loop(0, span // m_tile)
         def _(i):
             at = pl.ds(pl.multiple_of(i * m_tile, m_tile), m_tile)
-            for c in range(3):
-                at_c = pl.ds(c * cols, cols)
-                term = jnp.dot(normed[at, at_k], w_all[at_k, at_c], preferred_element_type=F32)
+            for c in range(count):
+                term = jnp.dot(normed[at, at_k], gather.buf[at_k, c * cols:(c + 1) * cols],
+                               preferred_element_type=F32)
+                at_c = pl.ds((first + c) * cols, cols)
                 acc[at, at_c] = term if t == 0 else acc[at, at_c] + term
 
+    cut = [blocks * i // layers for i in range(layers + 1)]
     for t in range(layers):
-        if t + 2 < layers:
-            gq.column(t + 2)
-        else:
-            go.column(t + 2 - layers)
+        lax.fori_loop(cut[t], cut[t + 1], trig, 0)
         if t + 1 < layers:
-            gq.cross(t + 1)
-        product(t)
+            gk.cross(t + 1)
+        if t + 3 < layers:
+            gk.column(t + 3)
+        if t == layers - 2:
+            gq.column(0)
+            gq.column(1)
+        product(gk, t, 1, 2)
+    gq.cross(0)
+    for t in range(2, layers):
+        gq.column(t)
+        gq.cross(t - 1)
 
     gap = (lax.broadcasted_iota(jnp.int32, (BLOCK, BLOCK), 0)
            - lax.broadcasted_iota(jnp.int32, (BLOCK, BLOCK), 1)).astype(F32)
@@ -243,12 +253,9 @@
         for h in range(heads):
             rate = rates[b, h]
             head = pl.ds(h * HEAD_DIM, HEAD_DIM)
-            u = acc[at, pl.ds(h * HEAD_DIM, HEAD_DIM)]
-            q = (u * cos + pltpu.roll(u, HEAD_DIM // 2, 1) * sin).astype(BF16)
             u = acc[at, pl.ds(cols + h * HEAD_DIM, HEAD_DIM)]
             k = (u * cos + pltpu.roll(u, HEAD_DIM // 2, 1) * sin).astype(BF16)
             v = acc[at, pl.ds(2 * cols + h * HEAD_DIM, HEAD_DIM)].astype(BF16)
-            q_rot[at, head] = q
             k_rot[at, head] = k
             v_row[at, head] = v
             tail = jnp.exp(-(BLOCK - 1.0 - row) * rate) * HEAD_DIM ** (-0.5)
@@ -290,16 +297,21 @@
 
     def inside(b, carry):
         at = pl.ds(pl.multiple_of(b * BLOCK, BLOCK), BLOCK)
+        cos, sin = cosine[at, :], sine[at, :]
         for h in range(heads):
             rate = rates[b, h]
             head = pl.ds(h * HEAD_DIM, HEAD_DIM)
+            u = acc[at, head]
+            q_rot[at, head] = (u * cos + pltpu.roll(u, HEAD_DIM // 2, 1) * sin).astype(BF16)
             fall = jnp.where(gap >= 0.0, jnp.exp(-jnp.maximum(gap, 0.0) * rate), 0.0)
             score = nt_dot(q_rot[at, head], k_rot[at, head]) * (fall * HEAD_DIM ** (-0.5))
             inner[at, head] = jnp.dot(score.astype(BF16), v_row[at, head], preferred_element_type=F32)
         return carry
 
-    third = -(-blocks // 3)
-    lax.fori_loop(0, third, inside, 0)
+    gq.cross(layers - 1)
+    go.column(0)
+    for t in range(layers // 2):
+        product(gq, t, 0, 1)
     for h in range(heads):
         pair(0, h, x_dev).wait_recv()
         got = take(0, h)
@@ -311,7 +323,10 @@
         own_decay = jnp.broadcast_to(decay, (8, HEAD_DIM))
         incoming[h, :8] = own_decay
         pair(1, h, y_dev).start()
-    lax.fori_loop(third, 2 * third, inside, 0)
+    go.column(1)
+    go.cross(0)
+    for t in range(layers // 2, layers):
+        product(gq, t, 0, 1)
     for h in range(heads):
         pair(1, h, y_dev).wait_recv()
         got = take(1, h)
@@ -320,32 +335,41 @@
         excl_d[h] = jnp.broadcast_to(jnp.where(y == 1, own_d * got[0], own_d), (8, HEAD_DIM))
         decay, value = both(y == 1, incoming[h, :8][:1], state[h], got)
         state[h] = value
-
-        def lift(h):
-            return remote(z_send.at[h], z_recv.at[h], zs_s.at[h], zs_r.at[h], up_dev)
-
-        @pl.when(z == 0)
-        def _():
-            incoming[h] = state_init[h]
-
-        @pl.when(z > 0)
-        def _():
-            lift(h).wait_recv()
-            incoming[h] = z_recv[h].astype(F32)
-
-        @pl.when(z < layers - 1)
-        def _():
-            z_send[h] = (decay * incoming[h] + value).astype(BF16)
-            lift(h).start()
-
-        incoming[h] = excl_d[h][:1] * incoming[h] + excl[h]
-
+        plane_d[h] = jnp.broadcast_to(decay, (8, HEAD_DIM))
+
+    def lift(h):
+        return remote(z_send.at[h], z_recv.at[h], zs_s.at[h], zs_r.at[h], up_dev)
+
+    def relay(from_below):
+        for h in range(heads):
+            if from_below:
+                lift(h).wait_recv()
+                incoming[h] = z_recv[h].astype(F32)
+            else:
+                incoming[h] = state_init[h]
+
+            @pl.when(z < layers - 1)
+            def _():
+                z_send[h] = (plane_d[h][:1] * incoming[h] + state[h]).astype(BF16)
+                lift(h).start()
+
+            incoming[h] = excl_d[h][:1] * incoming[h] + excl[h]
+
+    pl.when(z == 0)(lambda: relay(False))
+    if layers > 2:
+        go.column(2)
+        go.cross(1)
+    third = -(-blocks // 3)
+    lax.fori_loop(0, third, inside, 0)
+    pl.when(z == 1)(lambda: relay(True))
+    for t in range(3, layers):
+        go.column(t)
+        go.cross(t - 1)
+    lax.fori_loop(third, 2 * third, inside, 0)
+    pl.when(z == 2)(lambda: relay(True))
+    go.cross(layers - 1)
     lax.fori_loop(2 * third, blocks, inside, 0)
-
-    for t in range(layers):
-        if t + 2 < layers:
-            go.column(t + 2)
-        go.cross(t)
+    pl.when(z > 2)(lambda: relay(True))
 
     def finish(b, sums):
         at = pl.ds(pl.multiple_of(b * BLOCK, BLOCK), BLOCK)
@@ -401,6 +425,7 @@
             total = total + landed[d - 1, at, :].astype(F32)
         out[at, :] = total.astype(BF16)
 
+    gk.drain()
     gq.drain()
     go.drain()
     for d in range(1, peers):
@@ -440,7 +465,8 @@
         in_specs=[vmem, vmem, hbm, hbm, hbm, hbm, smem, vmem, vmem, vmem],
         out_specs=vmem,
         scratch_shapes=[
-            v((width, 3 * cols), BF16), v((width, cols), BF16), v((span, width), BF16),
+            v((width, 2 * cols), BF16), v((width, cols), BF16), v((width, cols), BF16),
+            v((span, width), BF16),
             v((span, 3 * cols), F32), v((span, HEAD_DIM), F32), v((span, HEAD_DIM), F32),
             v((span, cols), BF16), v((span, cols), BF16), v((span, cols), BF16),
             v((span, cols), F32), v((blocks, heads, HEAD_DIM, HEAD_DIM), F32),
@@ -449,11 +475,12 @@
             v((rows_here, width), BF16),
             v((2, heads, HEAD_DIM + 16, HEAD_DIM), BF16), v((2, heads, HEAD_DIM + 16, HEAD_DIM), BF16),
             v((heads, HEAD_DIM, HEAD_DIM), F32), v((heads, 8, HEAD_DIM), F32),
+            v((heads, 8, HEAD_DIM), F32),
             v((heads, HEAD_DIM, HEAD_DIM), BF16), v((heads, HEAD_DIM, HEAD_DIM), BF16),
             v((heads, HEAD_DIM, HEAD_DIM), F32),
             dma((4,)), dma((others,)), dma((others,)), dma((others,)), dma((others,)),
             dma((2, heads)), dma((2, heads)), dma((heads,)), dma((heads,)),
-        ] + gather_sems * 2,
+        ] + gather_sems * 3,
         compiler_params=pltpu.CompilerParams(
             collective_id=0, has_side_effects=True, vmem_limit_bytes=62 * 1024 * 1024),
     )(tokens, norm_gain[None], w_query, w_key, w_value, w_out.T, decay_rate, state_init,

time: 115 us -> 103 us (0.90)
  Pallas kernels: 108 us -> 95.6 us
    pallas_call x1, Pallas kernels: 108 us -> 95.6 us  [shards(): pl.pallas_call(functools.partial(kernel, layers, peers), out_shape=jax.Sh...]
where the time goes in v2:
time: 103 us; the launch traced here: 102 us
  Pallas kernels  95.6 us (93%)
  local copies, waits for them, and re-layouts  6.17 us (6%)
    pallas_call x1, Pallas kernels, shards(): pl.pallas_call(functools.partial(kernel, layers, peers), out_shape=jax.Sh...  95.6 us
    unnamed x3, local copies, waits for them, and re-layouts  6.17 us

profile of v2, /device:TPU:1, one launch (start us, length us, event | category | flops | bytes accessed | tf_op | source)
XLA Modules:
  0.0 102.4 jit_solution(3285745498919897319)
XLA Ops:
  0.0 0.6 maximum_bitcast_fusion.freq
  0.6 1.3 %copy.11.rates = f32[8,4]{1,0:T(8,128)} copy(f32[8,4]{0,1:T(4,128)} %param.14) | data formatting | bytes 256 | tf_op args[5]
  2.0 1.7 %copy.10 = bf16[512,128]{0,1:T(8,128)(2,1)} copy(bf16[512,128]{1,0:T(8,128)(2,1)} %param.17) | data formatting | bytes 262144 | tf_op args[8]
  3.6 95.6 %shard_map.91 = bf16[512,2048]{1,0:T(8,128)(2,1)} custom-call(bf16[512,2048]{1,0:T(8,128)(2,1)} %tokens.1, f32[1,2048]{1,0:T(1,128)} %bitcast.6, bf16[128,512]{1,0:T(8,128)(2,1)} %wq.1, bf16[128,512]{1,0:T(8,128)(2,1)} %wk.1, bf16[128,512]{1,0:T(8,128)(2,1)} %wv.1, bf16[128,512]{1,0:T(8,128)(2,1)} %bitcast.5, f32[8,4]{1,0:T(8,128)} %copy.11.rates, ...), custom_call_target="tpu_custom_call" | custom-call | tf_op jit(solution)/shard_map/pallas_call | solution.py:462
  99.3 3.2 %copy.13 = bf16[512,2048]{1,0:T(8,128)(2,1)} copy(bf16[512,2048]{1,0:T(8,128)(2,1)} %shard_map.91) | data formatting | bytes 4194304
  (1 shorter events, 0.0 us)
